TPU v7x, 32 devices: a whole 2x2x4 slice. The times are simulated.
32 devices in a mesh: st: 16 (over z, y, x), tp: 2 (over core).
Axes of the slice: x: 2, y: 2, z: 4, core: 2. Of those that a mesh axis runs over, the one named last changes fastest.
Arguments:
- tokens: bfloat16 [4096, 2048], P('st'), may hold values from -6 to 6
- store: bfloat16 [64, 64, 2048], P('st'), may hold values from -6 to 6
- passage_ids: int32 [64, 4], P('st'), may hold values from 0 to 63, as said below
- w_query: bfloat16 [2048, 2048], P(None, 'tp'), may hold values from -0.125 to 0.125
- w_key: bfloat16 [2048, 512], P(None, 'tp'), may hold values from -0.125 to 0.125
- w_value: bfloat16 [2048, 512], P(None, 'tp'), may hold values from -0.125 to 0.125
- w_ret_query: bfloat16 [2048, 1024], P(None, 'tp'), may hold values from -0.125 to 0.125
- w_ret_key: bfloat16 [2048, 1024], P(None, 'tp'), may hold values from -0.125 to 0.125
- w_ret_value: bfloat16 [2048, 2048], P(None, 'tp'), may hold values from -0.125 to 0.125
- ret_rate: float32 [8], P('tp'), may hold values from 0.003 to 0.03
- ret_gain: float32 [2048], P('tp'), may hold values from 0.1 to 1.9
- gate_logit: float32 [2048], P('tp'), may hold values from -2 to 2
- out_grad: bfloat16 [4096, 2048], P('st', 'tp'), may hold values from -6 to 6
Outputs:
- grad_tokens: bfloat16 [4096, 2048], P(('st', 'tp'))
- grad_store: bfloat16 [64, 64, 2048], P(('st', 'tp'))
- grad_key_weight: float32 [2048, 512], P(None, 'tp')
Inputs may be any that keep to these rules, and one draw needn't show every extreme that they name: `passage_ids`: passage p lies on index p // 4 of st. The rows of one device name exactly 1 passage of every owner, so the 4 passages of a block differ.
All inputs are finite; a program needn't handle non-finite values.
Results may differ from a plain program's by a relative error of at most 0.012.
Values may be sent and summed in bfloat16 or wider, within the bound.
A program may use at most 192 MiB of HBM per device.

v0:
```python
import jax
import jax.numpy as jnp
from jax import lax
from jax.sharding import PartitionSpec as P

HEAD = 256
BLK = 64
KP = 4
MOST = 1
EPSILON = 1.0


def retention_grads(query_rows, key_rows, value_rows, rates, gains, cotangent):
    length = query_rows.shape[0]
    heads = rates.shape[0]
    queries = query_rows.reshape(length, heads, -1)
    keyset = key_rows.reshape(length, heads, -1)
    values = value_rows.reshape(length, heads, -1)
    positions = jnp.arange(length, dtype=jnp.float32)
    distance = positions[:, None] - positions[None, :]
    damping = jnp.where(
        distance >= 0.0, jnp.exp(-rates[:, None, None] * jnp.maximum(distance, 0.0)), 0.0
    ) * queries.shape[-1] ** (-0.5)
    raw = jnp.einsum("thd,shd->hts", queries, keyset, preferred_element_type=jnp.float32)
    weights = (raw * damping).astype(jnp.bfloat16)
    mixed = jnp.einsum("hts,she->the", weights, values, preferred_element_type=jnp.float32)
    inverse = lax.rsqrt(jnp.mean(mixed * mixed, axis=-1, keepdims=True) + EPSILON)
    scaled = cotangent.astype(jnp.float32).reshape(length, heads, -1) * gains.reshape(heads, -1)
    inner = jnp.mean(scaled * mixed, axis=-1, keepdims=True)
    grad_mixed = (inverse * scaled - inverse * inverse * inverse * mixed * inner).astype(
        jnp.bfloat16
    )
    grad_weights = (
        jnp.einsum("the,she->hts", grad_mixed, values, preferred_element_type=jnp.float32) * damping
    ).astype(jnp.bfloat16)
    grad_first = (
        jnp.einsum("hts,shd->thd", grad_weights, keyset, preferred_element_type=jnp.float32)
        .astype(jnp.bfloat16)
        .reshape(length, -1)
    )
    grad_second = (
        jnp.einsum("hts,thd->shd", grad_weights, queries, preferred_element_type=jnp.float32)
        .astype(jnp.bfloat16)
        .reshape(length, -1)
    )
    grad_third = (
        jnp.einsum("hts,the->she", weights, grad_mixed, preferred_element_type=jnp.float32)
        .astype(jnp.bfloat16)
        .reshape(length, -1)
    )
    return (grad_first, grad_second, grad_third)


def against_rows(left, weight):
    return lax.dot_general(
        left, weight, (((1,), (1,)), ((), ())), preferred_element_type=jnp.float32
    )


def across_rows(left, right):
    return lax.dot_general(
        left, right, (((0,), (0,)), ((), ())), preferred_element_type=jnp.float32
    )


def per_device(
    tokens,
    store,
    passage_ids,
    w_query,
    w_key,
    w_value,
    w_ret_query,
    w_ret_key,
    w_ret_value,
    ret_rate,
    ret_gain,
    gate_logit,
    out_grad,
):
    owners = lax.axis_size("st")
    pass_dev, plen, width = store.shape
    length = tokens.shape[0]
    kv_width = w_key.shape[1]
    kv_local = kv_width // HEAD
    group = w_query.shape[1] // HEAD // kv_local
    blocks = length // BLK
    slot_ids = passage_ids.reshape(-1)
    slot_count = slot_ids.shape[0]
    slot_owner = slot_ids // pass_dev
    slot_local = slot_ids % pass_dev
    order = jnp.arange(slot_count, dtype=jnp.int32)
    same_owner = slot_owner[:, None] == slot_owner[None, :]
    rank = jnp.sum(same_owner & (order[None, :] < order[:, None]), axis=1)
    position = slot_owner * MOST + rank
    cells = owners * MOST
    placed = jnp.arange(cells, dtype=jnp.int32)[:, None] == position[None, :]
    request = (jnp.sum(jnp.where(placed, slot_local[None, :] + 1, 0), axis=1) - 1).reshape(
        owners, MOST
    )
    incoming = lax.all_to_all(request, "st", split_axis=0, concat_axis=0, tiled=True)
    wanted = incoming.reshape(-1)
    valid = wanted >= 0
    safe = jnp.maximum(wanted, 0)
    placed_bf = placed.astype(jnp.bfloat16)
    store_rows = store.reshape(-1, width)
    nothing = jnp.zeros((), jnp.bfloat16)
    own_kv = jnp.concatenate(
        [
            jnp.dot(store_rows, w_key, preferred_element_type=jnp.float32).astype(jnp.bfloat16),
            jnp.dot(store_rows, w_value, preferred_element_type=jnp.float32).astype(jnp.bfloat16),
        ],
        axis=1,
    ).reshape(pass_dev, plen, 2 * kv_width)
    reply = jnp.where(valid[:, None, None], own_kv[safe], nothing).reshape(
        owners, MOST, plen, 2 * kv_width
    )
    arrived = lax.all_to_all(reply, "st", split_axis=0, concat_axis=0, tiled=True)
    slot_kv = (
        across_rows(placed_bf, arrived.reshape(cells, -1))
        .astype(jnp.bfloat16)
        .reshape(slot_count, plen, 2 * kv_width)
    )
    factor = HEAD ** (-0.5)
    gate = jax.nn.sigmoid(gate_logit)
    query_bf = jnp.dot(tokens, w_query, preferred_element_type=jnp.float32).astype(jnp.bfloat16)
    queries = query_bf.reshape(blocks, BLK, kv_local, group, HEAD)
    keys = slot_kv[:, :, :kv_width].reshape(blocks, KP * plen, kv_local, HEAD)
    values = slot_kv[:, :, kv_width:].reshape(blocks, KP * plen, kv_local, HEAD)
    scores = (
        jnp.einsum("btkgd,bskd->bkgts", queries, keys, preferred_element_type=jnp.float32) * factor
    )
    expo = jnp.exp(scores)
    probs = expo / jnp.sum(expo, axis=-1, keepdims=True)
    probs_bf = probs.astype(jnp.bfloat16)
    attn = jnp.einsum("bkgts,bskd->btkgd", probs_bf, values, preferred_element_type=jnp.float32)
    grad_attn = out_grad.astype(jnp.float32).reshape(
        blocks, BLK, kv_local, group, HEAD
    ) * gate.reshape(kv_local, group, HEAD)
    grad_attn_bf = grad_attn.astype(jnp.bfloat16)
    grad_probs = jnp.einsum(
        "btkgd,bskd->bkgts", grad_attn_bf, values, preferred_element_type=jnp.float32
    )
    delta = jnp.moveaxis(jnp.sum(grad_attn * attn, axis=-1), 1, 3)
    grad_scores = (probs * (grad_probs - delta[..., None]) * factor).astype(jnp.bfloat16)
    grad_query = (
        jnp.einsum("bkgts,bskd->btkgd", grad_scores, keys, preferred_element_type=jnp.float32)
        .astype(jnp.bfloat16)
        .reshape(length, -1)
    )
    grad_keys = (
        jnp.einsum("bkgts,btkgd->bskd", grad_scores, queries, preferred_element_type=jnp.float32)
        .astype(jnp.bfloat16)
        .reshape(slot_count, plen, kv_width)
    )
    grad_values = (
        jnp.einsum("bkgts,btkgd->bskd", probs_bf, grad_attn_bf, preferred_element_type=jnp.float32)
        .astype(jnp.bfloat16)
        .reshape(slot_count, plen, kv_width)
    )
    slot_grad = jnp.concatenate([grad_keys, grad_values], axis=2)
    outgoing = (
        jnp.dot(placed_bf, slot_grad.reshape(slot_count, -1), preferred_element_type=jnp.float32)
        .astype(jnp.bfloat16)
        .reshape(owners, MOST, plen, 2 * kv_width)
    )
    returned = lax.all_to_all(outgoing, "st", split_axis=0, concat_axis=0, tiled=True)
    matched = (jnp.arange(pass_dev, dtype=jnp.int32)[:, None] == wanted[None, :]).astype(
        jnp.bfloat16
    )
    passage_grad = jnp.dot(
        matched, returned.reshape(cells, -1), preferred_element_type=jnp.float32
    ).reshape(pass_dev * plen, 2 * kv_width)
    key_grad = passage_grad[:, :kv_width]
    upper = key_grad.astype(jnp.bfloat16)
    lower = (key_grad - upper.astype(jnp.float32)).astype(jnp.bfloat16)
    key_term = across_rows(store_rows, upper) + across_rows(store_rows, lower)
    grad_key_weight = lax.psum(key_term, "st")
    passage_bf = passage_grad.astype(jnp.bfloat16)
    grad_store = lax.psum_scatter(
        (
            against_rows(passage_bf[:, :kv_width], w_key)
            + against_rows(passage_bf[:, kv_width:], w_value)
        ).astype(jnp.bfloat16),
        "tp",
        scatter_dimension=0,
        tiled=True,
    ).astype(jnp.float32)
    grad_store = grad_store.astype(jnp.bfloat16).reshape(-1, plen, width)
    ret_query = jnp.dot(tokens, w_ret_query, preferred_element_type=jnp.float32).astype(
        jnp.bfloat16
    )
    ret_key = jnp.dot(tokens, w_ret_key, preferred_element_type=jnp.float32).astype(jnp.bfloat16)
    ret_value = jnp.dot(tokens, w_ret_value, preferred_element_type=jnp.float32).astype(
        jnp.bfloat16
    )
    grad_rq, grad_rk, grad_rv = retention_grads(
        ret_query, ret_key, ret_value, ret_rate, ret_gain, out_grad
    )
    total = against_rows(grad_query, w_query)
    total = total + against_rows(grad_rq, w_ret_query)
    total = total + against_rows(grad_rk, w_ret_key)
    grad_tokens = lax.psum_scatter(
        (total + against_rows(grad_rv, w_ret_value)).astype(jnp.bfloat16),
        "tp",
        scatter_dimension=0,
        tiled=True,
    )
    return (grad_tokens, grad_store, grad_key_weight)


def solution(mesh):
    return jax.shard_map(
        per_device,
        mesh=mesh,
        in_specs=(
            P("st", None),
            P("st", None, None),
            P("st", None),
            P(None, "tp"),
            P(None, "tp"),
            P(None, "tp"),
            P(None, "tp"),
            P(None, "tp"),
            P(None, "tp"),
            P("tp"),
            P("tp"),
            P("tp"),
            P("st", "tp"),
        ),
        out_specs=(P(("st", "tp"), None), P(("st", "tp"), None, None), P(None, "tp")),
        check_vma=False,
    )
```

profile of v0, /device:TPU:0, one launch (start us, length us, event | category | flops | bytes accessed | tf_op | source)
XLA Modules:
  0.0 243.0 jit_solution(17686899952723807470)
XLA Ops:
  10.0 8.3 %all-to-all-start = ((s32[16,1,1]{2,1,0:T(1,128)}), s32[16,1,1]{2,1,0:T(1,128)S(1)}, u32[]{:S(2)}, u32[]{:S(2)}) async-start(s32[16,1,1]{2,1,0:T(1,128)} %copy.79), calls=%async_computation | async-start | bytes 16384 | tf_op jit(solution)/shard_map/all_to_all | solution.py:101
  18.3 2.1 convolution_convert_fusion.10
  22.9 2.7 %all-to-all-done = s32[16,1,1]{2,1,0:T(1,128)S(1)} async-done(((s32[16,1,1]{2,1,0:T(1,128)}), s32[16,1,1]{2,1,0:T(1,128)S(1)}, u32[]{:S(2)}, u32[]{:S(2)}) %all-to-all-start) | async-done | bytes 96 | tf_op jit(solution)/shard_map/all_to_all | solution.py:101
  28.2 2.4 fusion.18
  30.6 4.3 %all-to-all-start.1 = ((bf16[16,1,64,512]{3,2,1,0:T(8,128)(2,1)}), bf16[16,1,64,512]{3,2,1,0:T(8,128)(2,1)}, u32[]{:S(2)}, u32[]{:S(2)}) async-start(bf16[16,1,64,512]{3,2,1,0:T(8,128)(2,1)} %fusion.18), calls=%async_computation.1 | async-start | bytes 2097152 | tf_op jit(solution)/shard_map/all_to_all | solution.py:118
  34.9 2.2 copy.89
  37.2 2.5 %reshape.312 = f32[4,64,4,256]{3,2,1,0:T(4,128)} reshape(bf16[256,1024]{1,0:T(8,128)(2,1)} %param.25) | data formatting | bytes 1572864 | tf_op jit(solution)/shard_map/reshape | solution.py:137
  39.7 2.5 %reshape.313 = f32[4,64,1,4,256]{4,3,1,0,2:T(4,128)} reshape(bf16[256,1024]{1,0:T(8,128)(2,1)} %param.25) | data formatting | bytes 1572864 | tf_op jit(solution)/shard_map/reshape | solution.py:137
  42.2 1.9 convolution_convert_fusion.8
  45.0 3.3 %convolution_convert_fusion.9 = bf16[256,512]{1,0:T(8,128)(2,1)} fusion(bf16[256,2048]{1,0:T(8,128)(2,1)} %param.13, bf16[2048,512]{1,0:T(8,128)(2,1)} %param.20), kind=kOutput, calls=%fused_computation.40 | convolution fusion | flops 537001984 | bytes 3407872 | tf_op jit(solution)/shard_map/dot_general | solution.py:193
  49.4 4.6 %convolution_convert_fusion.5 = bf16[256,1024]{1,0:T(8,128)(2,1)} fusion(bf16[256,2048]{1,0:T(8,128)(2,1)} %param.13, bf16[2048,1024]{1,0:T(8,128)(2,1)} %param.16), kind=kOutput, calls=%fused_computation.33 | convolution fusion | flops 1074003968 | bytes 5767168 | tf_op jit(solution)/shard_map/dot_general | solution.py:126
  54.0 2.2 reshape.310
  58.7 1.8 copy.105
  68.2 6.0 %all-to-all-start.2 = ((bf16[16,1,64,512]{3,2,1,0:T(8,128)(2,1)}), bf16[16,1,64,512]{3,2,1,0:T(8,128)(2,1)}, u32[]{:S(2)}, u32[]{:S(2)}) async-start(bf16[16,1,64,512]{3,2,1,0:T(8,128)(2,1)} %bitcast.183), calls=%async_computation.3 | async-start | bytes 2097152 | tf_op jit(solution)/shard_map/all_to_all | solution.py:167
  75.9 4.0 %convolution_convert_fusion.4 = bf16[256,1024]{1,0:T(8,128)(2,1)S(1)} fusion(bf16[256,2048]{1,0:T(8,128)(2,1)} %param.13, bf16[2048,1024]{1,0:T(8,128)(2,1)} %param.21), kind=kOutput, calls=%fused_computation.32 | convolution fusion | flops 1074003968 | bytes 5767168 | tf_op jit(solution)/shard_map/dot_general | solution.py:194
  83.6 13.5 %all-to-all-done.2 = bf16[16,1,64,512]{3,2,1,0:T(8,128)(2,1)} async-done(((bf16[16,1,64,512]{3,2,1,0:T(8,128)(2,1)}), bf16[16,1,64,512]{3,2,1,0:T(8,128)(2,1)}, u32[]{:S(2)}, u32[]{:S(2)}) %all-to-all-start.2) | async-done | bytes 1048608 | tf_op jit(solution)/shard_map/all_to_all | solution.py:167
  97.2 1.8 copy.110
  100.1 2.2 reshape.329
  103.8 1.8 fusion.1
  107.4 3.7 %fusion.49 = f32[256,2048]{1,0:T(8,128)S(1)} fusion(bf16[256,1024]{0,1:T(8,128)(2,1)S(1)} %bitcast.195, bf16[2048,1024]{1,0:T(8,128)(2,1)} %param.21), kind=kOutput, calls=%fused_computation.101 | convolution fusion | flops 1073741824 | bytes 6815744 | tf_op jit(solution)/shard_map/dot_general | solution.py:55
  114.8 1.7 fusion.2
  116.7 1.8 fusion.34
  120.0 112.7 %all-reduce.2.cloned.1.call-done = f32[2048,256]{0,1:T(8,128)} async-done(((f32[2048,256]{0,1:T(8,128)}), f32[2048,256]{0,1:T(8,128)}) %all-reduce.2.cloned.1.call-update) | async-done | bytes 2097168 | tf_op jit(solution)/shard_map/psum | solution.py:178
  232.7 2.9 %copy.96 = f32[2048,256]{1,0:T(8,128)} copy(f32[2048,256]{0,1:T(8,128)} %all-reduce.2.cloned.1.call-done) | data formatting | bytes 4194304
  (114 shorter events, 34.1 us)
Async XLA Ops:
  8.0 34.2 %copy-start = (bf16[2048,512]{1,0:T(8,128)(2,1)S(1)}, bf16[2048,512]{1,0:T(8,128)(2,1)}, u32[]{:S(2)}) copy-start(bf16[2048,512]{1,0:T(8,128)(2,1)} %param.19) | copy-start | bytes 6291460
  8.0 12.5 %copy-start.1 = (bf16[4,64,2048]{2,1,0:T(8,128)(2,1)S(1)}, bf16[4,64,2048]{2,1,0:T(8,128)(2,1)}, u32[]{:S(2)}) copy-start(bf16[4,64,2048]{2,1,0:T(8,128)(2,1)} %param.14) | copy-start | bytes 3145732
  10.0 15.6 %all-to-all-start = ((s32[16,1,1]{2,1,0:T(1,128)}), s32[16,1,1]{2,1,0:T(1,128)S(1)}, u32[]{:S(2)}, u32[]{:S(2)}) async-start(s32[16,1,1]{2,1,0:T(1,128)} %copy.79), calls=%async_computation | async-start | bytes 16384 | tf_op jit(solution)/shard_map/all_to_all | solution.py:101
  18.3 2.2 copy-start.8
  30.6 28.1 %all-to-all-start.1 = ((bf16[16,1,64,512]{3,2,1,0:T(8,128)(2,1)}), bf16[16,1,64,512]{3,2,1,0:T(8,128)(2,1)}, u32[]{:S(2)}, u32[]{:S(2)}) async-start(bf16[16,1,64,512]{3,2,1,0:T(8,128)(2,1)} %fusion.18), calls=%async_computation.1 | async-start | bytes 2097152 | tf_op jit(solution)/shard_map/all_to_all | solution.py:118
  34.9 7.3 %copy-start.26 = (f32[4]{0:T(128)S(1)}, f32[4]{0:T(128)}, u32[]{:S(2)}) copy-start(f32[4]{0:T(128)} %param.22) | copy-start | bytes 52
  34.9 7.2 %copy-start.23 = (f32[1024]{0:T(1024)S(1)}, f32[1024]{0:T(1024)}, u32[]{:S(2)}) copy-start(f32[1024]{0:T(1024)} %param.23) | copy-start | bytes 12292
  34.9 7.2 %copy-start.24 = (f32[1024]{0:T(1024)S(1)}, f32[1024]{0:T(1024)}, u32[]{:S(2)}) copy-start(f32[1024]{0:T(1024)} %param.24) | copy-start | bytes 12292
  68.2 29.0 %all-to-all-start.2 = ((bf16[16,1,64,512]{3,2,1,0:T(8,128)(2,1)}), bf16[16,1,64,512]{3,2,1,0:T(8,128)(2,1)}, u32[]{:S(2)}, u32[]{:S(2)}) async-start(bf16[16,1,64,512]{3,2,1,0:T(8,128)(2,1)} %bitcast.183), calls=%async_computation.3 | async-start | bytes 2097152 | tf_op jit(solution)/shard_map/all_to_all | solution.py:167
  74.1 158.6 %all-reduce.2.cloned.1.call-start = ((), (), s32[]{:S(2)}) async-start(), calls=%async_computation.7 | async-start | bytes 4194304 | tf_op jit(solution)/shard_map/psum | solution.py:178
  75.9 4.0 %copy-start.14 = (bf16[4,256,256]{2,1,0:T(8,128)(2,1)}, bf16[4,256,256]{2,1,0:T(8,128)(2,1)S(1)}, u32[]{:S(2)}) copy-start(bf16[4,256,256]{2,1,0:T(8,128)(2,1)S(1)} %fusion.10) | copy-start | bytes 1572868
  75.9 4.0 %copy-start.2 = (f32[256,1024]{0,1:T(8,128)S(1)}, f32[256,1024]{0,1:T(8,128)}, u32[]{:S(2)}) copy-start(f32[256,1024]{0,1:T(8,128)} %copy.89) | copy-start | bytes 3145732
  102.3 1.5 copy-start.6
  105.5 1.5 copy-start.13
  105.5 1.5 copy-start.15
  105.6 130.0 %reduce-scatter.3.cloned.1.call-start = ((), (), s32[]{:S(2)}) async-start(), calls=%async_computation.5 | async-start | bytes 1572864 | tf_op jit(solution)/shard_map/reduce_scatter | solution.py:203
  107.4 3.7 %copy-start.5 = (bf16[16,64,256]{2,1,0:T(8,128)(2,1)S(1)}, bf16[16,64,256]{2,1,0:T(8,128)(2,1)}, u32[]{:S(2)}) copy-start(bf16[16,64,256]{2,1,0:T(8,128)(2,1)} %copy-done.4) | copy-start | bytes 1572868
  107.4 3.7 %copy-start.11 = (bf16[4,4,64,256]{3,2,1,0:T(8,128)(2,1)S(1)}, bf16[4,4,64,256]{3,2,1,0:T(8,128)(2,1)}, u32[]{:S(2)}) copy-start(bf16[4,4,64,256]{3,2,1,0:T(8,128)(2,1)} %copy-done.10) | copy-start | bytes 1572868
  107.4 4.5 %copy-start.25 = (bf16[2048,1024]{1,0:T(8,128)(2,1)S(1)}, bf16[2048,1024]{1,0:T(8,128)(2,1)}, u32[]{:S(2)}) copy-start(bf16[2048,1024]{1,0:T(8,128)(2,1)} %param.16) | copy-start | bytes 12582916
  113.2 1.6 copy-start.17
  113.3 1.6 copy-start.21
  114.8 1.8 copy-start.7
  116.6 119.0 %reduce-scatter.5.cloned.1.call-start = ((), (), s32[]{:S(2)}) async-start(), calls=%async_computation.6 | async-start | bytes 1572864 | tf_op jit(solution)/shard_map/reduce_scatter | solution.py:180
  116.7 1.8 copy-start.9
  (9 other events, 9.6 us)
Sparse Core Ops, SparseCore 0:
  105.7 126.9 all-reduce.1
Sparse Core Ops, SparseCore 1:
  116.7 8.7 reduce-scatter.2
  128.1 9.5 reduce-scatter.4
where the time goes:
time: 244 us; the launch traced here: 243 us
  waiting for transfers between devices  131 us (54%)
  matrix products  40.1 us (16%)
  local copies, waits for them, and re-layouts  31.6 us (13%)
  starting transfers between devices  19 us (8%)
  between operations  16 us (7%)
  other arithmetic  5.71 us (2%)
    psum x1, waiting for transfers between devices, per_device(): grad_key_weight = lax.psum(key_term, 'st')  113 us
    all_to_all x1, waiting for transfers between devices, per_device(): lax.all_to_all(outgoing, 'st', split_axis=0, concat_axis=0, tiled=True)  13.5 us
    unnamed x61, local copies, waits for them, and re-layouts  13.2 us
    dot_general x6, matrix products, against_rows(): lax.dot_general(left, weight, (((1,), (1,)), ((), ())), preferred_element...  10.7 us
    all_to_all x1, starting transfers between devices, per_device(): lax.all_to_all(request, 'st', split_axis=0, concat_axis=0, tiled=True)  8.34 us
    all_to_all x1, starting transfers between devices, per_device(): lax.all_to_all(outgoing, 'st', split_axis=0, concat_axis=0, tiled=True)  5.96 us
    reshape x2, local copies, waits for them, and re-layouts, per_device(): out_grad.astype(jnp.float32).reshape(blocks, BLK, kv_local, group, HEAD)  4.98 us
  transfers between devices with their start and end apart: 6, of which 4 were waited for; matrix products, arithmetic and copies ran while one was open for 21% of the time, Pallas kernels for 0%

commit v1 on v0

--- a/solution.py
+++ b/solution.py
@@ -175,7 +175,7 @@
     upper = key_grad.astype(jnp.bfloat16)
     lower = (key_grad - upper.astype(jnp.float32)).astype(jnp.bfloat16)
     key_term = across_rows(store_rows, upper) + across_rows(store_rows, lower)
-    grad_key_weight = lax.psum(key_term, "st")
+    grad_key_weight = jnp.sum(lax.all_gather(key_term, "st"), axis=0)
     passage_bf = passage_grad.astype(jnp.bfloat16)
     grad_store = lax.psum_scatter(
         (

time: 244 us -> 505 us (2.07)
  waiting for transfers between devices: 131 us -> 335 us
  blocking collectives: 0 us -> 30.7 us
  local copies, waits for them, and re-layouts: 31.6 us -> 58.8 us
  other arithmetic: 5.71 us -> 14.4 us
  starting transfers between devices: 19 us -> 13 us
    all_gather x0 -> x1, waiting for transfers between devices: none -> 321 us  [per_device(): grad_key_weight = jnp.sum(lax.all_gather(key_term, 'st'), axis=0)]
    psum x1 -> x0, waiting for transfers between devices: 113 us -> none  [per_device(): grad_key_weight = lax.psum(key_term, 'st')]
    all_to_all x0 -> x1, blocking collectives: none -> 30.7 us  [per_device(): lax.all_to_all(outgoing, 'st', split_axis=0, concat_axis=0, tiled=True)]
    unnamed x61 -> x54, local copies, waits for them, and re-layouts: 13.2 us -> 40.3 us
    all_to_all x1 -> x0, waiting for transfers between devices: 13.5 us -> none  [per_device(): lax.all_to_all(outgoing, 'st', split_axis=0, concat_axis=0, tiled=True)]
    all_to_all x1, waiting for transfers between devices: 1.66 us -> 11.9 us  [per_device(): lax.all_to_all(reply, 'st', split_axis=0, concat_axis=0, tiled=True)]
    reduce_sum x0 -> x1, other arithmetic: none -> 9.41 us  [per_device(): grad_key_weight = jnp.sum(lax.all_gather(key_term, 'st'), axis=0)]
    all_to_all x1 -> x0, starting transfers between devices: 5.96 us -> none  [per_device(): lax.all_to_all(outgoing, 'st', split_axis=0, concat_axis=0, tiled=True)]
  transfers between devices with their start and end apart: 6 -> 5, of which waited for: 4 -> 3; matrix products, arithmetic and copies ran while one was open for 21% -> 17% of each run, Pallas kernels for 0% -> 0%
where the time goes in v1:
time: 505 us; the launch traced here: 504 us
  waiting for transfers between devices  335 us (66%)
  local copies, waits for them, and re-layouts  58.8 us (12%)
  matrix products  35.5 us (7%)
  blocking collectives  30.7 us (6%)
  between operations  16 us (3%)
  other arithmetic  14.4 us (3%)
  starting transfers between devices  13 us (3%)
    all_gather x1, waiting for transfers between devices, per_device(): grad_key_weight = jnp.sum(lax.all_gather(key_term, 'st'), axis=0)  321 us
    unnamed x54, local copies, waits for them, and re-layouts  40.3 us
    all_to_all x1, blocking collectives, per_device(): lax.all_to_all(outgoing, 'st', split_axis=0, concat_axis=0, tiled=True)  30.7 us
    all_to_all x1, waiting for transfers between devices, per_device(): lax.all_to_all(reply, 'st', split_axis=0, concat_axis=0, tiled=True)  11.9 us
  transfers between devices with their start and end apart: 5, of which 3 were waited for; matrix products, arithmetic and copies ran while one was open for 17% of the time, Pallas kernels for 0%

profile of v1, /device:TPU:0, one launch (start us, length us, event | category | flops | bytes accessed | tf_op | source)
XLA Modules:
  0.0 503.7 jit_solution(15763105106193943301)
XLA Ops:
  10.0 8.3 %all-to-all-start = ((s32[16,1,1]{2,1,0:T(1,128)}), s32[16,1,1]{2,1,0:T(1,128)S(1)}, u32[]{:S(2)}, u32[]{:S(2)}) async-start(s32[16,1,1]{2,1,0:T(1,128)} %copy.77), calls=%async_computation | async-start | bytes 16384 | tf_op jit(solution)/shard_map/all_to_all | solution.py:101
  18.3 2.1 convolution_convert_fusion.10
  22.9 2.7 all-to-all-done
  26.2 1.6 gather_fusion
  28.2 2.3 fusion.18
  30.5 4.3 all-to-all-start.1
  35.0 2.5 reshape.312
  37.5 2.5 reshape.313
  40.0 4.6 convolution_convert_fusion.5
  44.6 2.2 reshape.310
  46.8 11.9 %all-to-all-done.1 = bf16[16,1,64,512]{3,2,1,0:T(8,128)(2,1)} async-done(((bf16[16,1,64,512]{3,2,1,0:T(8,128)(2,1)}), bf16[16,1,64,512]{3,2,1,0:T(8,128)(2,1)}, u32[]{:S(2)}, u32[]{:S(2)}) %all-to-all-start.1) | async-done | bytes 1048608 | tf_op jit(solution)/shard_map/all_to_all | solution.py:118
  58.7 1.8 copy.103
  67.1 30.7 %all_to_all.16 = bf16[16,1,64,512]{3,2,1,0:T(8,128)(2,1)S(1)} all-to-all(bf16[16,1,64,512]{3,2,1,0:T(8,128)(2,1)S(1)} %bitcast.192), channel_id=1, replica_groups=mesh['st'=16,'tp'=2] {'st'}, dimensions={0} | all-to-all | bytes 2097152 | tf_op jit(solution)/shard_map/all_to_all | solution.py:167
  99.5 2.2 reshape.329
  103.2 1.8 fusion.1
  106.4 2.6 convolution_convert_fusion.8
  110.1 3.9 convolution_convert_fusion.9
  114.0 1.8 copy.100
  117.5 3.5 convolution_convert_fusion.4
  129.4 1.7 fusion.2
  134.4 320.7 %all-gather.3.cloned.1.call-done = f32[32768,256]{0,1:T(8,128)} async-done(((f32[2048,256]{0,1:T(8,128)}), f32[32768,256]{0,1:T(8,128)}) %all-gather.3.cloned.1.call-update) | async-done | bytes 33554448 | tf_op jit(solution)/shard_map/all_gather | solution.py:178
  455.1 28.8 %copy.109 = f32[32,8,16,2048]{3,2,1,0:T(8,128)S(1)} copy(f32[32,8,16,2048]{3,1,2,0:T(8,128)} %bitcast.176) | data formatting | bytes 67108864
  483.9 9.4 %bitcast_reduce_fusion = f32[2048,256]{0,1:T(8,128)} fusion(f32[32,8,16,2048]{3,2,1,0:T(8,128)S(1)} %copy.109), kind=kLoop, calls=%fused_computation.3 | loop fusion | flops 7864320 | bytes 35651584 | tf_op jit(solution)/shard_map/reduce_sum | solution.py:178
  493.3 2.9 copy.94
  (107 shorter events, 30.6 us)
Async XLA Ops:
  8.0 98.4 %copy-start = (bf16[2048,512]{1,0:T(8,128)(2,1)S(1)}, bf16[2048,512]{1,0:T(8,128)(2,1)}, u32[]{:S(2)}) copy-start(bf16[2048,512]{1,0:T(8,128)(2,1)} %param.19) | copy-start | bytes 6291460
  8.0 12.5 %copy-start.2 = (bf16[4,64,2048]{2,1,0:T(8,128)(2,1)S(1)}, bf16[4,64,2048]{2,1,0:T(8,128)(2,1)}, u32[]{:S(2)}) copy-start(bf16[4,64,2048]{2,1,0:T(8,128)(2,1)} %param.14) | copy-start | bytes 3145732
  10.0 15.6 %all-to-all-start = ((s32[16,1,1]{2,1,0:T(1,128)}), s32[16,1,1]{2,1,0:T(1,128)S(1)}, u32[]{:S(2)}, u32[]{:S(2)}) async-start(s32[16,1,1]{2,1,0:T(1,128)} %copy.77), calls=%async_computation | async-start | bytes 16384 | tf_op jit(solution)/shard_map/all_to_all | solution.py:101
  18.3 2.2 copy-start.8
  30.5 28.1 %all-to-all-start.1 = ((bf16[16,1,64,512]{3,2,1,0:T(8,128)(2,1)}), bf16[16,1,64,512]{3,2,1,0:T(8,128)(2,1)}, u32[]{:S(2)}, u32[]{:S(2)}) async-start(bf16[16,1,64,512]{3,2,1,0:T(8,128)(2,1)} %fusion.18), calls=%async_computation.1 | async-start | bytes 2097152 | tf_op jit(solution)/shard_map/all_to_all | solution.py:118
  34.9 5.1 %copy-start.17 = (f32[1024]{0:T(1024)S(1)}, f32[1024]{0:T(1024)}, u32[]{:S(2)}) copy-start(f32[1024]{0:T(1024)} %param.24) | copy-start | bytes 12292
  34.9 420.2 %all-gather.3.cloned.1.call-start = ((), (), s32[]{:S(2)}) async-start(), calls=%async_computation.7 | async-start | bytes 35651584 | tf_op jit(solution)/shard_map/all_gather | solution.py:178
  61.0 1.2 copy-start.3
  61.3 1.5 copy-start.14
  101.7 1.5 copy-start.6
  105.0 1.3 copy-start.22
  105.0 1.4 copy-start.18
  105.0 391.2 %reduce-scatter.3.cloned.1.call-start = ((), (), s32[]{:S(2)}) async-start(), calls=%async_computation.5 | async-start | bytes 1572864 | tf_op jit(solution)/shard_map/reduce_scatter | solution.py:203
  115.9 1.6 copy-start.21
  121.7 2.3 copy-start.19
  124.0 1.3 copy-start.5
  124.0 1.3 copy-start.12
  124.0 2.5 copy-start.20
  127.8 1.6 copy-start.13
  129.4 2.0 copy-start.7
  131.2 1.2 copy-start.9
  131.2 365.0 %reduce-scatter.5.cloned.1.call-start = ((), (), s32[]{:S(2)}) async-start(), calls=%async_computation.6 | async-start | bytes 1572864 | tf_op jit(solution)/shard_map/reduce_scatter | solution.py:180
  131.5 1.4 copy-start.10
  483.9 12.3 %copy-start.1 = (bf16[2048,512]{1,0:T(8,128)(2,1)S(1)}, bf16[2048,512]{1,0:T(8,128)(2,1)}, u32[]{:S(2)}) copy-start(bf16[2048,512]{1,0:T(8,128)(2,1)} %param.19) | copy-start | bytes 6291460
  (4 other events, 3.8 us)
Sparse Core Ops, SparseCore 0:
  105.2 349.9 all-gather.2
Sparse Core Ops, SparseCore 1:
  131.3 6.8 reduce-scatter.2
  140.8 9.5 reduce-scatter.4
